TPU v7x, 128 devices: a whole 4x4x4 slice. The times are simulated.
128 devices in a mesh: sp: 32 (over z, y, core), tp: 4 (over x).
Axes of the slice: x: 4, y: 4, z: 4, core: 2. Of those that a mesh axis runs over, the one named last changes fastest.
Arguments:
- query_rows: bfloat16 [32768, 1024], P('sp', 'tp'), may hold values from -6 to 6
- key_rows: bfloat16 [32768, 1024], P('sp', 'tp'), may hold values from -6 to 6
- value_rows: bfloat16 [32768, 1024], P('sp', 'tp'), may hold values from -6 to 6
- input_gate: float32 [8, 32768], P('tp', 'sp'), may hold values from -4 to 255
- forget_gate: float32 [8, 32768], P('tp', 'sp'), may hold values from -3 to 20
- output_gate: bfloat16 [32768, 1024], P('sp', 'tp'), may hold values from -6 to 6
- documents: int32 [32768], P('sp'), may hold values from 0 to 7, never falling along the last dimension, each value on 1 to 6144 neighbouring positions
- residual: bfloat16 [32768, 2048], P(('sp', 'tp')), may hold values from -6 to 6
- out_weight: bfloat16 [1024, 2048], P('tp'), may hold values from -0.375 to 0.375
- norm_gain: bfloat16 [2048], replicated, may hold values from 0.099609375 to 1.8984375
- gate_weight: bfloat16 [2048, 5632], P('sp', 'tp'), may hold values from -0.125 to 0.125
- up_weight: bfloat16 [2048, 5632], P('sp', 'tp'), may hold values from -0.125 to 0.125
- down_weight: bfloat16 [5632, 2048], P('tp', 'sp'), may hold values from -0.15625 to 0.15625
Outputs:
- layer_out: bfloat16 [32768, 2048], P(('sp', 'tp'))
Inputs may be any that keep to these rules, and one draw needn't show every extreme that they name: `documents`: document numbers never fall along the positions; each document covers 1 to 6144 positions and one covers exactly 6144.
All inputs are finite; a program needn't handle non-finite values.
Results may differ from a plain program's by a relative error of at most 0.013.
Values may be sent and summed in bfloat16 or wider, within the bound.
A program may use at most 128 MiB of HBM per device.

v0:
```python
import jax
import jax.numpy as jnp
from jax import lax
from jax.sharding import Mesh
from jax.sharding import PartitionSpec as P

HD = 128
BLOCK = 128
SP = ("sp_0", "sp_1", "sp_2")
SP_TP = ("sp_0", "sp_1", "sp_2", "tp")
neg_large = -1e30
norm_eps = 1e-06
highest = lax.Precision.HIGHEST


def gather_turned(arrays, axis, dims):
    turned = [jnp.moveaxis(a, dim, 0) for a, dim in zip(arrays, dims)]
    both = jnp.concatenate([t.reshape(len(t), -1) for t in turned], axis=1)
    whole, at, finished = (lax.all_gather(both, axis, axis=0, tiled=True), 0, [])
    for t, dim in zip(turned, dims):
        slab = whole[:, at : at + t[0].size].reshape(-1, *t.shape[1:])
        finished.append(jnp.moveaxis(slab, 0, dim))
        at += t[0].size
    return tuple(finished)


def nothing_yet(array, identity):
    return jax.tree.map(
        lambda part, zero: jnp.zeros_like(part) + jnp.asarray(zero, part.dtype), array, identity
    )


def all_in_one(array, axis):
    leaves = jax.tree.leaves(array)
    sequence = sorted(range(len(leaves)), key=lambda k: -leaves[k].size)
    width = (1, *leaves[sequence[0]].shape)[-1]
    lines = [
        jnp.pad(leaves[k].reshape(-1), (0, -leaves[k].size % width)).reshape(-1, width)
        for k in sequence
    ]
    both, at, found = (lax.all_gather(jnp.concatenate(lines), axis), 0, {})
    for k, line in zip(sequence, lines):
        slab = both[:, at : at + len(line)].reshape(len(both), -1)
        found[k] = slab[:, : leaves[k].size].reshape(-1, *leaves[k].shape)
        at += len(line)
    numbers = iter(range(len(leaves)))
    return jax.tree.map(lambda _: found[next(numbers)], array)


def gathered_by_type(array, axis):
    leaves, found = (jax.tree.leaves(array), {})
    for leading, a in enumerate(leaves):
        if leading not in found:
            alike = [k for k, b in enumerate(leaves) if b.dtype == a.dtype]
            got = (
                all_in_one([leaves[k] for k in alike], axis)
                if len(alike) > 1
                else [lax.all_gather(a, axis)]
            )
            for k, b in zip(alike, got):
                found[k] = b
    numbers = iter(range(len(leaves)))
    return jax.tree.map(lambda _: found[next(numbers)], array)


def prefix_by_axis(array, axes, combine, identity):
    before = start = nothing_yet(array, identity)
    total = array
    for axis in reversed(axes):
        devices, position = (lax.axis_size(axis), lax.axis_index(axis))
        pieces = gathered_by_type(total, axis)
        inside, total = (start, start)
        for k in range(devices):
            passed = k < position
            total = combine(total, jax.tree.map(lambda part: part[k], pieces))
            inside = jax.tree.map(lambda new, old: jnp.where(passed, new, old), total, inside)
        before = combine(inside, before)
    return before


def block_step(carried, inputs):
    memory, normer, stab_prev, carry_doc = carried
    queries, key_float, value_float, gate_in, log_forget, docs = inputs
    cumlog = jnp.cumsum(log_forget, axis=1)
    length = docs.shape[0]
    target_positions = jnp.arange(length)
    same_doc = (docs[:, None] == docs[None, :]) & (
        target_positions[:, None] >= target_positions[None, :]
    )
    log_weight = jnp.where(
        same_doc[None], cumlog[:, :, None] - cumlog[:, None, :] + gate_in[:, None, :], neg_large
    )
    carried_log = jnp.where((docs == carry_doc)[None, :], cumlog + stab_prev[:, None], neg_large)
    stabilizer = jnp.maximum(carried_log, jnp.max(log_weight, axis=2))
    scores = jnp.einsum("lhd,shd->hls", queries, key_float, precision=highest)
    weighted = scores * jnp.exp(log_weight - stabilizer[:, :, None])
    carried_scale = jnp.exp(carried_log - stabilizer)
    numerator = carried_scale[:, :, None] * jnp.einsum(
        "lhd,hde->hle", queries, memory, precision=highest
    )
    numerator = numerator + jnp.einsum("hls,she->hle", weighted, value_float, precision=highest)
    denominator = carried_scale * jnp.einsum(
        "lhd,hd->hl", queries, normer, precision=highest
    ) + jnp.sum(weighted, axis=2)
    outputs = numerator / jnp.maximum(jnp.abs(denominator), 1.0)[:, :, None]
    last_doc = docs[-1]
    inject_log = jnp.where(
        (docs == last_doc)[None, :], cumlog[:, -1:] - cumlog + gate_in, neg_large
    )
    inject_max = jnp.max(inject_log, axis=1)
    weights = jnp.exp(inject_log - inject_max[:, None])
    continues = carry_doc == last_doc
    stab_new = jnp.where(continues, jnp.maximum(cumlog[:, -1] + stab_prev, inject_max), inject_max)
    decay_scale = jnp.where(continues, jnp.exp(cumlog[:, -1] + stab_prev - stab_new), 0.0)
    inject = jnp.exp(inject_max - stab_new)
    memory_step = jnp.einsum(
        "lhd,lhe->hde", key_float * weights.T[:, :, None], value_float, precision=highest
    )
    normer_step = jnp.einsum("hl,lhd->hd", weights, key_float, precision=highest)
    memory = decay_scale[:, None, None] * memory + inject[:, None, None] * memory_step
    normer = decay_scale[:, None] * normer + inject[:, None] * normer_step
    return ((memory, normer, stab_new, last_doc), jnp.transpose(outputs, (1, 0, 2)))


def run_blocks(queries, key_float, value_float, gate_in, log_forget, docs, start_state):
    length, heads, width = queries.shape
    count = length // BLOCK
    inputs = (
        queries.reshape(count, BLOCK, heads, width),
        key_float.reshape(count, BLOCK, heads, width),
        value_float.reshape(count, BLOCK, heads, width),
        jnp.moveaxis(gate_in.reshape(heads, count, BLOCK), 1, 0),
        jnp.moveaxis(log_forget.reshape(heads, count, BLOCK), 1, 0),
        docs.reshape(count, BLOCK),
    )
    final, outputs = lax.scan(block_step, start_state, inputs)
    return (outputs.reshape(length, heads, width), final)


def join_states(earlier, later_part):
    memory_early, normer_early, stab_early, total_early, doc_early = earlier
    memory_late, normer_late, stab_late, total_late, doc_late = later_part
    continues = doc_late == doc_early
    is_empty = doc_late < 0
    stab_both = jnp.where(continues, jnp.maximum(total_late + stab_early, stab_late), stab_late)
    scale_early = jnp.where(continues, jnp.exp(total_late + stab_early - stab_both), 0.0)
    scale_late = jnp.exp(stab_late - stab_both)
    memory = scale_early[:, None, None] * memory_early + scale_late[:, None, None] * memory_late
    normer = scale_early[:, None] * normer_early + scale_late[:, None] * normer_late
    return (
        jnp.where(is_empty, memory_early, memory),
        jnp.where(is_empty, normer_early, normer),
        jnp.where(is_empty, stab_early, stab_both),
        total_early + total_late,
        jnp.where(is_empty, doc_early, doc_late),
    )


def body(
    query_rows,
    key_rows,
    value_rows,
    input_gate,
    forget_gate,
    output_gate,
    documents,
    residual,
    out_weight,
    norm_gain,
    gate_weight,
    up_weight,
    down_weight,
):
    whole_gate, whole_up, whole_down = gather_turned(
        (gate_weight, up_weight, down_weight), SP, (0, 0, 1)
    )
    tokens = query_rows.shape[0]
    local_heads = input_gate.shape[0]
    queries = query_rows.astype(jnp.float32).reshape(tokens, local_heads, HD) * HD ** (-0.5)
    key_float = key_rows.astype(jnp.float32).reshape(tokens, local_heads, HD)
    value_float = value_rows.astype(jnp.float32).reshape(tokens, local_heads, HD)
    log_forget = jax.nn.log_sigmoid(forget_gate)
    cumlog = jnp.cumsum(log_forget, axis=1)
    total = cumlog[:, -1]
    last_doc = documents[-1]
    inject_log = jnp.where(
        (documents == last_doc)[None, :], total[:, None] - cumlog + input_gate, neg_large
    )
    inject_max = jnp.max(inject_log, axis=1)
    weights = jnp.exp(inject_log - inject_max[:, None])
    memory = jnp.einsum(
        "thd,the->hde", key_float * weights.T[:, :, None], value_float, precision=highest
    )
    normer = jnp.einsum("ht,thd->hd", weights, key_float, precision=highest)
    identity = (
        jnp.zeros_like(memory),
        jnp.zeros_like(normer),
        jnp.full_like(inject_max, neg_large),
        jnp.zeros_like(total),
        jnp.array(-1, jnp.int32),
    )
    before = prefix_by_axis(
        (memory, normer, inject_max, total, last_doc), SP, join_states, identity
    )
    cells, final = run_blocks(
        queries,
        key_float,
        value_float,
        input_gate,
        log_forget,
        documents,
        (before[0], before[1], before[2], before[4]),
    )
    gated = (cells.reshape(tokens, -1) * jax.nn.sigmoid(output_gate.astype(jnp.float32))).astype(
        jnp.bfloat16
    )
    mine = lax.all_to_all(gated, "tp", split_axis=0, concat_axis=1, tiled=True)
    projected = jnp.dot(
        mine,
        lax.all_gather(out_weight, "tp", axis=0, tiled=True),
        preferred_element_type=jnp.float32,
    )
    stream = residual.astype(jnp.float32) + projected
    normed = stream * lax.rsqrt(jnp.mean(stream * stream, axis=1, keepdims=True) + norm_eps)
    normed = (normed * norm_gain.astype(jnp.float32)).astype(jnp.bfloat16)
    rows_all = lax.all_gather(normed, "tp", axis=0, tiled=True)
    gate_act = jnp.dot(rows_all, whole_gate, preferred_element_type=jnp.float32)
    up_act = jnp.dot(rows_all, whole_up, preferred_element_type=jnp.float32)
    hidden = (jax.nn.silu(gate_act) * up_act).astype(jnp.bfloat16)
    partial_sum = jnp.dot(hidden, whole_down, preferred_element_type=jnp.float32)
    down = lax.psum_scatter(
        partial_sum.astype(jnp.bfloat16), "tp", scatter_dimension=0, tiled=True
    ).astype(jnp.float32)
    return (stream + 0.5 * down).astype(jnp.bfloat16)


def solution(mesh):
    torus = Mesh(mesh.devices.reshape(4, 4, 2, mesh.shape["tp"]), ("sp_0", "sp_1", "sp_2", "tp"))
    in_specs = (
        P(SP, "tp"),
        P(SP, "tp"),
        P(SP, "tp"),
        P("tp", SP),
        P("tp", SP),
        P(SP, "tp"),
        P(SP),
        P(SP_TP, None),
        P("tp", None),
        P(),
        P(SP, "tp"),
        P(SP, "tp"),
        P("tp", SP),
    )
    out_specs = P(SP_TP, None)
    return jax.shard_map(body, mesh=torus, in_specs=in_specs, out_specs=out_specs, check_vma=False)
```

profile of v0, /device:TPU:1, one launch (start us, length us, event | category | flops | bytes accessed | tf_op | source)
XLA Modules:
  0.0 448.9 jit_solution(14347902271754953552)
XLA Ops:
  8.7 1.2 dynamic-slice
  10.0 1.9 slice_dynamic-update-slice_fusion
  11.9 1.3 broadcast_compare_fusion
  15.4 1.2 copy.56
  16.7 1.4 fusion.34
  18.0 1.7 fusion.32
  19.8 3.2 all-gather.3
  23.6 1.8 all-reduce.6
  31.0 11.8 %all-gather.4 = f32[4,260,128]{2,1,0:T(8,128)S(1)} all-gather(f32[1,260,128]{2,1,0:T(8,128)S(1)} %maximum_bitcast_fusion.1), channel_id=3, replica_groups=mesh['sp_0'=4,'sp_1'=4,'sp_2'=2,'tp'=4] {'sp_1'}, dimensions={0}, use_global_device_ids=true | all-gather | bytes 665600 | tf_op jit(solution)/shard_map/all_gather | solution.py:41
  45.5 6.5 %all-reduce.7 = s32[4]{0:T(128)S(1)} all-reduce(s32[4]{0:T(128)S(1)} %dynamic-update-slice.1), channel_id=1, replica_groups=mesh['sp_0'=4,'sp_1'=4,'sp_2'=2,'tp'=4] {'sp_1'}, use_global_device_ids=true, to_apply=%add.7 | all-reduce | flops 4 | bytes 32
  61.6 11.7 %all-gather.5 = f32[4,260,128]{2,1,0:T(8,128)S(1)} all-gather(f32[1,260,128]{2,1,0:T(8,128)S(1)} %maximum_bitcast_fusion.2), channel_id=4, replica_groups=mesh['sp_0'=4,'sp_1'=4,'sp_2'=2,'tp'=4] {'sp_0'}, dimensions={0}, use_global_device_ids=true | all-gather | bytes 665600 | tf_op jit(solution)/shard_map/all_gather | solution.py:41
  74.2 1.5 reshape.2044
  75.6 1.2 dynamic-slice.2
  77.6 7.2 %all-reduce.8 = s32[4]{0:T(128)S(1)} all-reduce(s32[4]{0:T(128)S(1)} %dynamic-update-slice.2), channel_id=1, replica_groups=mesh['sp_0'=4,'sp_1'=4,'sp_2'=2,'tp'=4] {'sp_0'}, use_global_device_ids=true, to_apply=%add.8 | all-reduce | flops 4 | bytes 32
  92.9 1.1 convert_multiply_fusion
  94.1 1.5 reshape.2046
  95.9 1.8 add_select_fusion.3
  97.7 112.4 %while.18 = (s32[]{:T(128)}, f32[2,128,128]{2,1,0:T(8,128)S(1)}, f32[2,128]{1,0:T(2,128)S(1)}, f32[2]{0:T(128)S(1)}, s32[]{:T(128)}, /*index=5*/f32[8,128,2,128]...) while((s32[]{:T(128)}, f32[2,128,128]{2,1,0:T(8,128)S(1)}, ...), condition=%wide.region_8.9_spmd, body=%wide.region_3.8_spmd.sunk | while | flops 202756624 | bytes 3499011 | solution.py:136
  102.2 0.9 constant_dynamic-slice_fusion.10
  103.3 0.9 constant_dynamic-slice_fusion.9
  106.4 4.7 %dynamic_update_slice.5 = f32[8,128,2,128]{1,0,3,2:T(8,128)} dynamic-update-slice(f32[8,128,2,128]{1,0,3,2:T(8,128)} %get-tuple-element.360, f32[1,128,2,128]{1,0,3,2:T(1,128)S(1)} %copy.134, s32[]{:T(128)S(6)} %copy.145, s32[]{:T(128)} %constant.31.clone.1..sunk, s32[]{:T(128)} %constant.31.clone.1..sunk, s32[]{:T(128)} %constant.31.clone.1..sunk) | dynamic-update-slice | bytes 262148 | tf_op jit(solution)/shard_map/while/body/jit(dynamic_update_index_in_dim)/dynamic_update_slice | solution.py:136
  116.2 0.9 constant_dynamic-slice_fusion.10
  117.3 0.9 constant_dynamic-slice_fusion.9
  120.5 4.7 %dynamic_update_slice.5 = f32[8,128,2,128]{1,0,3,2:T(8,128)} dynamic-update-slice(f32[8,128,2,128]{1,0,3,2:T(8,128)} %get-tuple-element.360, f32[1,128,2,128]{1,0,3,2:T(1,128)S(1)} %copy.134, s32[]{:T(128)S(6)} %copy.145, s32[]{:T(128)} %constant.31.clone.1..sunk, s32[]{:T(128)} %constant.31.clone.1..sunk, s32[]{:T(128)} %constant.31.clone.1..sunk) | dynamic-update-slice | bytes 262148 | tf_op jit(solution)/shard_map/while/body/jit(dynamic_update_index_in_dim)/dynamic_update_slice | solution.py:136
  130.2 0.9 constant_dynamic-slice_fusion.10
  131.4 0.9 constant_dynamic-slice_fusion.9
  134.5 4.7 %dynamic_update_slice.5 = f32[8,128,2,128]{1,0,3,2:T(8,128)} dynamic-update-slice(f32[8,128,2,128]{1,0,3,2:T(8,128)} %get-tuple-element.360, f32[1,128,2,128]{1,0,3,2:T(1,128)S(1)} %copy.134, s32[]{:T(128)S(6)} %copy.145, s32[]{:T(128)} %constant.31.clone.1..sunk, s32[]{:T(128)} %constant.31.clone.1..sunk, s32[]{:T(128)} %constant.31.clone.1..sunk) | dynamic-update-slice | bytes 262148 | tf_op jit(solution)/shard_map/while/body/jit(dynamic_update_index_in_dim)/dynamic_update_slice | solution.py:136
  145.4 0.9 constant_dynamic-slice_fusion.9
  148.6 4.7 %dynamic_update_slice.5 = f32[8,128,2,128]{1,0,3,2:T(8,128)} dynamic-update-slice(f32[8,128,2,128]{1,0,3,2:T(8,128)} %get-tuple-element.360, f32[1,128,2,128]{1,0,3,2:T(1,128)S(1)} %copy.134, s32[]{:T(128)S(6)} %copy.145, s32[]{:T(128)} %constant.31.clone.1..sunk, s32[]{:T(128)} %constant.31.clone.1..sunk, s32[]{:T(128)} %constant.31.clone.1..sunk) | dynamic-update-slice | bytes 262148 | tf_op jit(solution)/shard_map/while/body/jit(dynamic_update_index_in_dim)/dynamic_update_slice | solution.py:136
  159.5 0.9 constant_dynamic-slice_fusion.9
  162.6 4.7 %dynamic_update_slice.5 = f32[8,128,2,128]{1,0,3,2:T(8,128)} dynamic-update-slice(f32[8,128,2,128]{1,0,3,2:T(8,128)} %get-tuple-element.360, f32[1,128,2,128]{1,0,3,2:T(1,128)S(1)} %copy.134, s32[]{:T(128)S(6)} %copy.145, s32[]{:T(128)} %constant.31.clone.1..sunk, s32[]{:T(128)} %constant.31.clone.1..sunk, s32[]{:T(128)} %constant.31.clone.1..sunk) | dynamic-update-slice | bytes 262148 | tf_op jit(solution)/shard_map/while/body/jit(dynamic_update_index_in_dim)/dynamic_update_slice | solution.py:136
  173.5 0.9 constant_dynamic-slice_fusion.9
  176.6 4.7 %dynamic_update_slice.5 = f32[8,128,2,128]{1,0,3,2:T(8,128)} dynamic-update-slice(f32[8,128,2,128]{1,0,3,2:T(8,128)} %get-tuple-element.360, f32[1,128,2,128]{1,0,3,2:T(1,128)S(1)} %copy.134, s32[]{:T(128)S(6)} %copy.145, s32[]{:T(128)} %constant.31.clone.1..sunk, s32[]{:T(128)} %constant.31.clone.1..sunk, s32[]{:T(128)} %constant.31.clone.1..sunk) | dynamic-update-slice | bytes 262148 | tf_op jit(solution)/shard_map/while/body/jit(dynamic_update_index_in_dim)/dynamic_update_slice | solution.py:136
  187.6 0.9 constant_dynamic-slice_fusion.9
  190.7 4.7 %dynamic_update_slice.5 = f32[8,128,2,128]{1,0,3,2:T(8,128)} dynamic-update-slice(f32[8,128,2,128]{1,0,3,2:T(8,128)} %get-tuple-element.360, f32[1,128,2,128]{1,0,3,2:T(1,128)S(1)} %copy.134, s32[]{:T(128)S(6)} %copy.145, s32[]{:T(128)} %constant.31.clone.1..sunk, s32[]{:T(128)} %constant.31.clone.1..sunk, s32[]{:T(128)} %constant.31.clone.1..sunk) | dynamic-update-slice | bytes 262148 | tf_op jit(solution)/shard_map/while/body/jit(dynamic_update_index_in_dim)/dynamic_update_slice | solution.py:136
  201.6 0.9 constant_dynamic-slice_fusion.9
  204.7 4.7 %dynamic_update_slice.5 = f32[8,128,2,128]{1,0,3,2:T(8,128)} dynamic-update-slice(f32[8,128,2,128]{1,0,3,2:T(8,128)} %get-tuple-element.360, f32[1,128,2,128]{1,0,3,2:T(1,128)S(1)} %copy.134, s32[]{:T(128)S(6)} %copy.145, s32[]{:T(128)} %constant.31.clone.1..sunk, s32[]{:T(128)} %constant.31.clone.1..sunk, s32[]{:T(128)} %constant.31.clone.1..sunk) | dynamic-update-slice | bytes 262148 | tf_op jit(solution)/shard_map/while/body/jit(dynamic_update_index_in_dim)/dynamic_update_slice | solution.py:136
  210.4 1.6 fusion.31
  212.8 3.7 all-to-all-start
  216.5 6.9 %all-to-all-done = bf16[4,256,256]{1,2,0:T(8,128)(2,1)S(1)} async-done(((bf16[4,256,256]{1,2,0:T(8,128)(2,1)}), bf16[4,256,256]{1,2,0:T(8,128)(2,1)S(1)}, u32[]{:S(2)}, u32[]{:S(2)}) %all-to-all-start) | async-done | bytes 524320 | tf_op jit(solution)/shard_map/all_to_all | solution.py:217
  223.4 3.9 multiply_reduce_fusion
  227.4 1.2 multiply_convert_fusion.1
  229.8 52.7 %all-gather.12.cloned.1.call-done = bf16[1024,2048]{1,0:T(8,128)(2,1)} async-done(((bf16[256,2048]{1,0:T(8,128)(2,1)}), bf16[1024,2048]{1,0:T(8,128)(2,1)}) %all-gather.12.cloned.1.call-update) | async-done | bytes 4194320 | tf_op jit(solution)/shard_map/all_gather | solution.py:226
  282.5 77.2 %all-gather.14.cloned.1.call-done = bf16[2048,4224]{1,0:T(8,128)(2,1)} async-done(((bf16[64,4224]{1,0:T(8,128)(2,1)}), bf16[2048,4224]{1,0:T(8,128)(2,1)}) %all-gather.14.cloned.1.call-update) | async-done | bytes 17301520 | tf_op jit(solution)/shard_map/all_gather | solution.py:19
  359.6 11.7 %fusion.21 = f32[1024,1408]{1,0:T(8,128)} fusion(bf16[1024,2048]{1,0:T(8,128)(2,1)} %all-gather.12.cloned.1.call-done, bf16[2048,4224]{1,0:T(8,128)(2,1)} %all-gather.14.cloned.1.call-done), kind=kOutput, calls=%fused_computation.48 | convolution fusion | flops 5905580032 | bytes 15728640 | tf_op jit(solution)/shard_map/dot_general | solution.py:227
  371.3 22.7 %fusion.25 = bf16[1024,2048]{1,0:T(8,128)(2,1)} fusion(bf16[2048,4224]{1,0:T(8,128)(2,1)} %all-gather.14.cloned.1.call-done, f32[1024,1408]{1,0:T(8,128)} %fusion.21, bf16[1024,2048]{1,0:T(8,128)(2,1)} %all-gather.12.cloned.1.call-done), kind=kOutput, calls=%fused_computation.51 | convolution fusion | flops 11821907968 | bytes 25690112 | tf_op jit(solution)/shard_map/dot_general | solution.py:230
  394.0 45.9 %reduce-scatter.2.cloned.1.call-done = bf16[256,2048]{1,0:T(8,128)(2,1)} async-done(((bf16[1024,2048]{1,0:T(8,128)(2,1)}), bf16[256,2048]{1,0:T(8,128)(2,1)}) %reduce-scatter.2.cloned.1.call-update) | async-done | bytes 1048592 | tf_op jit(solution)/shard_map/reduce_scatter | solution.py:231
  439.9 2.5 add_convert_fusion
  (279 shorter events, 69.0 us)
Async XLA Ops:
  6.5 37.1 %copy-start.9 = (u32[128]{0:T(128)S(1)}, u32[128]{0:T(128)}, u32[]{:S(2)}) copy-start(u32[128]{0:T(128)} %constant.104) | copy-start | bytes 1540
  6.5 38.5 %copy-start.1 = (bf16[1024,256]{1,0:T(8,128)(2,1)S(1)}, bf16[1024,256]{1,0:T(8,128)(2,1)}, u32[]{:S(2)}) copy-start(bf16[1024,256]{1,0:T(8,128)(2,1)} %param.17) | copy-start | bytes 1572868
  6.5 216.9 %all-gather.10.cloned.1.call-start = ((), (), s32[]{:S(2)}) async-start(), calls=%async_computation.2 | async-start | bytes 5242880 | tf_op jit(solution)/shard_map/all_gather | solution.py:220
  19.7 54.4 %copy-start = (bf16[1024,256]{1,0:T(8,128)(2,1)S(1)}, bf16[1024,256]{1,0:T(8,128)(2,1)}, u32[]{:S(2)}) copy-start(bf16[1024,256]{1,0:T(8,128)(2,1)} %param.16) | copy-start | bytes 1572868
  30.2 0.5 copy-start.7
  60.6 0.6 copy-start.8
  97.7 112.4 %copy-start.2 = (bf16[1024,256]{1,0:T(8,128)(2,1)S(1)}, bf16[1024,256]{1,0:T(8,128)(2,1)}, u32[]{:S(2)}) copy-start(bf16[1024,256]{1,0:T(8,128)(2,1)} %param.20) | copy-start | bytes 1572868
  210.1 6.4 %copy-start.6 = (bf16[2048]{0:T(1024)(128)(2,1)S(1)}, bf16[2048]{0:T(1024)(128)(2,1)}, u32[]{:S(2)}) copy-start(bf16[2048]{0:T(1024)(128)(2,1)} %param.24) | copy-start | bytes 12292
  212.8 10.7 %all-to-all-start = ((bf16[4,256,256]{1,2,0:T(8,128)(2,1)}), bf16[4,256,256]{1,2,0:T(8,128)(2,1)S(1)}, u32[]{:S(2)}, u32[]{:S(2)}) async-start(bf16[4,256,256]{1,2,0:T(8,128)(2,1)} %bitcast.516), calls=%async_computation | async-start | bytes 1048576 | tf_op jit(solution)/shard_map/all_to_all | solution.py:217
  216.5 66.0 %all-gather.12.cloned.1.call-start = ((), (), s32[]{:S(2)}) async-start(), calls=%async_computation.3 | async-start | bytes 5242880 | tf_op jit(solution)/shard_map/all_gather | solution.py:226
  227.3 1.3 copy-start.3
  227.3 1.3 copy-start.4
  227.3 1.3 copy-start.5
  228.6 131.1 %all-gather.14.cloned.1.call-start = ((), (), s32[]{:S(2)}) async-start(), calls=%async_computation.4 | async-start | bytes 17842176 | tf_op jit(solution)/shard_map/all_gather | solution.py:19
  229.5 210.4 %reduce-scatter.2.cloned.1.call-start = ((), (), s32[]{:S(2)}) async-start(), calls=%async_computation.5 | async-start | bytes 5242880 | tf_op jit(solution)/shard_map/reduce_scatter | solution.py:231
Sparse Core Ops, SparseCore 0:
  9.0 51.1 all-gather.9
  228.7 53.7 all-gather.11
  284.7 74.8 all-gather.13
  394.2 45.7 reduce-scatter.1
where the time goes:
time: 451 us; the launch traced here: 449 us
  waiting for transfers between devices  183 us (41%)
  local copies, waits for them, and re-layouts  78.3 us (17%)
  matrix products  58.1 us (13%)
  blocking collectives  42.2 us (9%)
  other arithmetic  39.2 us (9%)
  between operations  32.8 us (7%)
  loops' own time  10.8 us (2%)
    all_gather x1, waiting for transfers between devices, gather_turned(): lax.all_gather(both, axis, axis=0, tiled=True)  77.2 us
    all_gather x1, waiting for transfers between devices, body(): rows_all = lax.all_gather(normed, 'tp', axis=0, tiled=True)  52.7 us
    reduce_scatter x1, waiting for transfers between devices, body(): lax.psum_scatter(partial_sum.astype(jnp.bfloat16), 'tp', scatter_dimensio...  45.9 us
    dynamic_update_slice x16, local copies, waits for them, and re-layouts, run_blocks(): final, outputs = lax.scan(block_step, start_state, inputs)  38.7 us
    all_gather x3, blocking collectives, all_in_one(): both, at, found = (lax.all_gather(jnp.concatenate(lines), axis), 0, {})  26.6 us
    dot_general x1, matrix products, body(): jnp.dot(hidden, whole_down, preferred_element_type=jnp.float32)  22.7 us
    unnamed x3, blocking collectives  15.6 us
    dynamic_slice x16, local copies, waits for them, and re-layouts, run_blocks(): final, outputs = lax.scan(block_step, start_state, inputs)  14.8 us
  transfers between devices with their start and end apart: 5, of which 4 were waited for; matrix products, arithmetic and copies ran while one was open for 30% of the time, Pallas kernels for 0%

commit v1 on v0

--- a/solution.py
+++ b/solution.py
@@ -223,7 +223,12 @@
     stream = residual.astype(jnp.float32) + projected
     normed = stream * lax.rsqrt(jnp.mean(stream * stream, axis=1, keepdims=True) + norm_eps)
     normed = (normed * norm_gain.astype(jnp.float32)).astype(jnp.bfloat16)
-    rows_all = lax.all_gather(normed, "tp", axis=0, tiled=True)
+    ring = [normed]
+    for hop in range(3):
+        ring.append(lax.ppermute(ring[-1], "tp", [(dev, (dev + 1) % 4) for dev in range(4)]))
+    rows_all = jnp.roll(
+        jnp.concatenate(ring[::-1], axis=0), (lax.axis_index("tp") + 1) * ring[0].shape[0], axis=0
+    )
     gate_act = jnp.dot(rows_all, whole_gate, preferred_element_type=jnp.float32)
     up_act = jnp.dot(rows_all, whole_up, preferred_element_type=jnp.float32)
     hidden = (jax.nn.silu(gate_act) * up_act).astype(jnp.bfloat16)

time: 451 us -> 396 us (0.88)
  waiting for transfers between devices: 183 us -> 123 us
  local copies, waits for them, and re-layouts: 78.3 us -> 83.6 us
    all_gather x1, waiting for transfers between devices: 77.2 us -> 0.01 us  [gather_turned(): lax.all_gather(both, axis, axis=0, tiled=True)]
    ppermute x0 -> x3, waiting for transfers between devices: none -> 60.5 us  [body(): lax.ppermute(ring[-1], 'tp', [(dev, (dev + 1) % 4) for dev in range(4)])]
    all_gather x1 -> x0, waiting for transfers between devices: 52.7 us -> none  [body(): rows_all = lax.all_gather(normed, 'tp', axis=0, tiled=True)]
    unnamed x31 -> x35, local copies, waits for them, and re-layouts: 7.75 us -> 20.2 us
    reduce_scatter x1, waiting for transfers between devices: 45.9 us -> 54.6 us  [body(): lax.psum_scatter(partial_sum.astype(jnp.bfloat16), 'tp', scatter_dimensio...]
    dynamic_slice x16, local copies, waits for them, and re-layouts: 14.8 us -> 8.17 us  [run_blocks(): final, outputs = lax.scan(block_step, start_state, inputs)]
  transfers between devices with their start and end apart: 5 -> 7, of which waited for: 4 -> 5; matrix products, arithmetic and copies ran while one was open for 30% -> 37% of each run, Pallas kernels for 0% -> 0%
where the time goes in v1:
time: 396 us; the launch traced here: 393 us
  waiting for transfers between devices  123 us (31%)
  local copies, waits for them, and re-layouts  83.6 us (21%)
  matrix products  56.2 us (14%)
  blocking collectives  43.8 us (11%)
  other arithmetic  41 us (10%)
  between operations  32.1 us (8%)
  loops' own time  9.67 us (2%)
  starting transfers between devices  4.11 us (1%)
    ppermute x3, waiting for transfers between devices, body(): lax.ppermute(ring[-1], 'tp', [(dev, (dev + 1) % 4) for dev in range(4)])  60.5 us
    reduce_scatter x1, waiting for transfers between devices, body(): lax.psum_scatter(partial_sum.astype(jnp.bfloat16), 'tp', scatter_dimensio...  54.6 us
    dynamic_update_slice x16, local copies, waits for them, and re-layouts, run_blocks(): final, outputs = lax.scan(block_step, start_state, inputs)  38.9 us
    all_gather x3, blocking collectives, all_in_one(): both, at, found = (lax.all_gather(jnp.concatenate(lines), axis), 0, {})  26 us
    dot_general x1, matrix products, body(): jnp.dot(hidden, whole_down, preferred_element_type=jnp.float32)  20.6 us
    unnamed x35, local copies, waits for them, and re-layouts  20.2 us
    unnamed x3, blocking collectives  17.9 us
    dot_general x1, matrix products, body(): gate_act = jnp.dot(rows_all, whole_gate, preferred_element_type=jnp.float32)  11.7 us
  transfers between devices with their start and end apart: 7, of which 5 were waited for; matrix products, arithmetic and copies ran while one was open for 37% of the time, Pallas kernels for 0%

profile of v1, /device:TPU:1, one launch (start us, length us, event | category | flops | bytes accessed | tf_op | source)
XLA Modules:
  0.0 393.3 jit_solution(17342517165000882984)
XLA Ops:
  7.3 1.9 pad_maximum_fusion
  9.3 1.3 dynamic-slice
  10.6 1.9 slice_dynamic-update-slice_fusion
  12.5 2.9 all-reduce.6
  17.9 1.2 dynamic-slice.1
  21.6 7.2 %all-reduce.7 = s32[4]{0:T(128)S(1)} all-reduce(s32[4]{0:T(128)S(1)} %dynamic-update-slice.1), channel_id=1, replica_groups=mesh['sp_0'=4,'sp_1'=4,'sp_2'=2,'tp'=4] {'sp_1'}, use_global_device_ids=true, to_apply=%add.7 | all-reduce | flops 4 | bytes 32
  36.8 1.3 broadcast_compare_fusion
  41.0 1.3 copy.56
  42.3 1.4 fusion.40
  43.7 1.7 fusion.38
  45.5 3.9 all-gather.3
  49.8 10.8 %all-gather.4 = f32[4,260,128]{2,1,0:T(8,128)S(1)} all-gather(f32[1,260,128]{2,1,0:T(8,128)S(1)} %maximum_bitcast_fusion.1), channel_id=3, replica_groups=mesh['sp_0'=4,'sp_1'=4,'sp_2'=2,'tp'=4] {'sp_1'}, dimensions={0}, use_global_device_ids=true | all-gather | bytes 665600 | tf_op jit(solution)/shard_map/all_gather | solution.py:41
  61.1 11.3 %all-gather.5 = f32[4,260,128]{2,1,0:T(8,128)S(1)} all-gather(f32[1,260,128]{2,1,0:T(8,128)S(1)} %maximum_bitcast_fusion.2), channel_id=4, replica_groups=mesh['sp_0'=4,'sp_1'=4,'sp_2'=2,'tp'=4] {'sp_0'}, dimensions={0}, use_global_device_ids=true | all-gather | bytes 665600 | tf_op jit(solution)/shard_map/all_gather | solution.py:41
  76.2 1.5 reshape.2045
  79.1 7.8 %all-reduce.8 = s32[4]{0:T(128)S(1)} all-reduce(s32[4]{0:T(128)S(1)} %dynamic-update-slice.2), channel_id=1, replica_groups=mesh['sp_0'=4,'sp_1'=4,'sp_2'=2,'tp'=4] {'sp_0'}, use_global_device_ids=true, to_apply=%add.8 | all-reduce | flops 4 | bytes 32
  95.1 1.1 convert_multiply_fusion
  96.3 1.5 reshape.2046
  97.7 1.4 copy.45
  100.2 1.7 add_select_fusion.3
  101.9 103.5 %while.18 = (s32[]{:T(128)}, f32[2,128,128]{2,1,0:T(8,128)S(1)}, f32[2,128]{1,0:T(2,128)S(1)}, f32[2]{0:T(128)S(1)}, s32[]{:T(128)}, /*index=5*/f32[8,128,2,128]...) while((s32[]{:T(128)}, f32[2,128,128]{2,1,0:T(8,128)S(1)}, ...), condition=%wide.region_8.9_spmd, body=%wide.region_3.8_spmd.sunk | while | flops 202756624 | bytes 3499003 | solution.py:136
  108.9 4.8 %dynamic_update_slice.5 = f32[8,128,2,128]{1,0,3,2:T(8,128)} dynamic-update-slice(f32[8,128,2,128]{1,0,3,2:T(8,128)} %get-tuple-element.360, f32[1,128,2,128]{1,0,3,2:T(1,128)S(1)} %copy.134, s32[]{:T(128)} %get-tuple-element.355, s32[]{:T(128)} %constant.61.clone.1..sunk, s32[]{:T(128)} %constant.61.clone.1..sunk, s32[]{:T(128)} %constant.61.clone.1..sunk) | dynamic-update-slice | bytes 262148 | tf_op jit(solution)/shard_map/while/body/jit(dynamic_update_index_in_dim)/dynamic_update_slice | solution.py:136
  121.9 4.8 %dynamic_update_slice.5 = f32[8,128,2,128]{1,0,3,2:T(8,128)} dynamic-update-slice(f32[8,128,2,128]{1,0,3,2:T(8,128)} %get-tuple-element.360, f32[1,128,2,128]{1,0,3,2:T(1,128)S(1)} %copy.134, s32[]{:T(128)} %get-tuple-element.355, s32[]{:T(128)} %constant.61.clone.1..sunk, s32[]{:T(128)} %constant.61.clone.1..sunk, s32[]{:T(128)} %constant.61.clone.1..sunk) | dynamic-update-slice | bytes 262148 | tf_op jit(solution)/shard_map/while/body/jit(dynamic_update_index_in_dim)/dynamic_update_slice | solution.py:136
  132.2 1.1 constant_dynamic-slice_fusion.9
  134.9 4.8 %dynamic_update_slice.5 = f32[8,128,2,128]{1,0,3,2:T(8,128)} dynamic-update-slice(f32[8,128,2,128]{1,0,3,2:T(8,128)} %get-tuple-element.360, f32[1,128,2,128]{1,0,3,2:T(1,128)S(1)} %copy.134, s32[]{:T(128)} %get-tuple-element.355, s32[]{:T(128)} %constant.61.clone.1..sunk, s32[]{:T(128)} %constant.61.clone.1..sunk, s32[]{:T(128)} %constant.61.clone.1..sunk) | dynamic-update-slice | bytes 262148 | tf_op jit(solution)/shard_map/while/body/jit(dynamic_update_index_in_dim)/dynamic_update_slice | solution.py:136
  147.9 4.7 %dynamic_update_slice.5 = f32[8,128,2,128]{1,0,3,2:T(8,128)} dynamic-update-slice(f32[8,128,2,128]{1,0,3,2:T(8,128)} %get-tuple-element.360, f32[1,128,2,128]{1,0,3,2:T(1,128)S(1)} %copy.134, s32[]{:T(128)} %get-tuple-element.355, s32[]{:T(128)} %constant.61.clone.1..sunk, s32[]{:T(128)} %constant.61.clone.1..sunk, s32[]{:T(128)} %constant.61.clone.1..sunk) | dynamic-update-slice | bytes 262148 | tf_op jit(solution)/shard_map/while/body/jit(dynamic_update_index_in_dim)/dynamic_update_slice | solution.py:136
  160.8 4.7 %dynamic_update_slice.5 = f32[8,128,2,128]{1,0,3,2:T(8,128)} dynamic-update-slice(f32[8,128,2,128]{1,0,3,2:T(8,128)} %get-tuple-element.360, f32[1,128,2,128]{1,0,3,2:T(1,128)S(1)} %copy.134, s32[]{:T(128)} %get-tuple-element.355, s32[]{:T(128)} %constant.61.clone.1..sunk, s32[]{:T(128)} %constant.61.clone.1..sunk, s32[]{:T(128)} %constant.61.clone.1..sunk) | dynamic-update-slice | bytes 262148 | tf_op jit(solution)/shard_map/while/body/jit(dynamic_update_index_in_dim)/dynamic_update_slice | solution.py:136
  173.7 4.7 %dynamic_update_slice.5 = f32[8,128,2,128]{1,0,3,2:T(8,128)} dynamic-update-slice(f32[8,128,2,128]{1,0,3,2:T(8,128)} %get-tuple-element.360, f32[1,128,2,128]{1,0,3,2:T(1,128)S(1)} %copy.134, s32[]{:T(128)} %get-tuple-element.355, s32[]{:T(128)} %constant.61.clone.1..sunk, s32[]{:T(128)} %constant.61.clone.1..sunk, s32[]{:T(128)} %constant.61.clone.1..sunk) | dynamic-update-slice | bytes 262148 | tf_op jit(solution)/shard_map/while/body/jit(dynamic_update_index_in_dim)/dynamic_update_slice | solution.py:136
  186.6 4.7 %dynamic_update_slice.5 = f32[8,128,2,128]{1,0,3,2:T(8,128)} dynamic-update-slice(f32[8,128,2,128]{1,0,3,2:T(8,128)} %get-tuple-element.360, f32[1,128,2,128]{1,0,3,2:T(1,128)S(1)} %copy.134, s32[]{:T(128)} %get-tuple-element.355, s32[]{:T(128)} %constant.61.clone.1..sunk, s32[]{:T(128)} %constant.61.clone.1..sunk, s32[]{:T(128)} %constant.61.clone.1..sunk) | dynamic-update-slice | bytes 262148 | tf_op jit(solution)/shard_map/while/body/jit(dynamic_update_index_in_dim)/dynamic_update_slice | solution.py:136
  199.5 4.7 %dynamic_update_slice.5 = f32[8,128,2,128]{1,0,3,2:T(8,128)} dynamic-update-slice(f32[8,128,2,128]{1,0,3,2:T(8,128)} %get-tuple-element.360, f32[1,128,2,128]{1,0,3,2:T(1,128)S(1)} %copy.134, s32[]{:T(128)} %get-tuple-element.355, s32[]{:T(128)} %constant.61.clone.1..sunk, s32[]{:T(128)} %constant.61.clone.1..sunk, s32[]{:T(128)} %constant.61.clone.1..sunk) | dynamic-update-slice | bytes 262148 | tf_op jit(solution)/shard_map/while/body/jit(dynamic_update_index_in_dim)/dynamic_update_slice | solution.py:136
  205.4 1.6 fusion.37
  207.8 3.7 all-to-all-start
  211.6 6.9 %all-to-all-done = bf16[4,256,256]{1,2,0:T(8,128)(2,1)S(1)} async-done(((bf16[4,256,256]{1,2,0:T(8,128)(2,1)}), bf16[4,256,256]{1,2,0:T(8,128)(2,1)S(1)}, u32[]{:S(2)}, u32[]{:S(2)}) %all-to-all-start) | async-done | bytes 524320 | tf_op jit(solution)/shard_map/all_to_all | solution.py:217
  218.5 3.9 multiply_reduce_fusion
  223.0 17.1 %collective-permute-done = bf16[256,2048]{1,0:T(8,128)(2,1)S(1)} collective-permute-done((bf16[256,2048]{1,0:T(8,128)(2,1)S(1)}, bf16[256,2048]{1,0:T(8,128)(2,1)S(1)}, u32[]{:S(2)}, u32[]{:S(2)}) %collective-permute-start) | collective-permute-done | bytes 1048608 | tf_op jit(solution)/shard_map/ppermute | solution.py:228
  240.1 21.7 %collective-permute-done.1 = bf16[256,2048]{1,0:T(8,128)(2,1)} collective-permute-done((bf16[256,2048]{1,0:T(8,128)(2,1)S(1)}, bf16[256,2048]{1,0:T(8,128)(2,1)}, u32[]{:S(2)}, u32[]{:S(2)}) %collective-permute-start.1) | collective-permute-done | bytes 1048608 | tf_op jit(solution)/shard_map/ppermute | solution.py:228
  261.8 21.6 %collective-permute-done.2 = bf16[256,2048]{1,0:T(8,128)(2,1)} collective-permute-done((bf16[256,2048]{1,0:T(8,128)(2,1)}, bf16[256,2048]{1,0:T(8,128)(2,1)}, u32[]{:S(2)}, u32[]{:S(2)}) %collective-permute-start.2) | collective-permute-done | bytes 1048608 | tf_op jit(solution)/shard_map/ppermute | solution.py:228
  283.4 2.3 constant_dynamic-update-slice_fusion.7
  285.8 2.3 constant_dynamic-update-slice_fusion.6
  288.1 1.0 constant_dynamic-update-slice_fusion.5
  289.1 1.2 constant_dynamic-update-slice_fusion.4
  290.4 2.3 constant_dynamic-update-slice_fusion.3
  292.7 2.3 constant_dynamic-update-slice_fusion.2
  295.0 1.0 constant_dynamic-update-slice_fusion.1
  296.0 1.3 constant_dynamic-update-slice_fusion
  297.3 11.7 %fusion.21 = f32[1024,1408]{1,0:T(8,128)} fusion(bf16[2048,4224]{1,0:T(8,128)(2,1)} %all-gather.11.cloned.1.call-done, bf16[2048,2048]{1,0:T(8,128)(2,1)} %constant_dynamic-update-slice_fusion, s32[]{:T(128)S(6)} %select_n.2247), kind=kOutput, calls=%fused_computation.48 | convolution fusion | flops 5905580032 | bytes 15728644 | tf_op jit(solution)/shard_map/dot_general | solution.py:232
  309.0 20.6 %fusion.23 = bf16[1024,2048]{1,0:T(8,128)(2,1)} fusion(bf16[2048,4224]{1,0:T(8,128)(2,1)} %all-gather.11.cloned.1.call-done, f32[1024,1408]{1,0:T(8,128)} %fusion.21, bf16[2048,2048]{1,0:T(8,128)(2,1)} %constant_dynamic-update-slice_fusion, s32[]{:T(128)S(6)} %select_n.2247), kind=kOutput, calls=%fused_computation.51 | convolution fusion | flops 11821907968 | bytes 25690116 | tf_op jit(solution)/shard_map/dot_general | solution.py:235
  329.7 54.6 %reduce-scatter.2.cloned.1.call-done = bf16[256,2048]{1,0:T(8,128)(2,1)} async-done(((bf16[1024,2048]{1,0:T(8,128)(2,1)}), bf16[256,2048]{1,0:T(8,128)(2,1)}) %reduce-scatter.2.cloned.1.call-update) | async-done | bytes 1048592 | tf_op jit(solution)/shard_map/reduce_scatter | solution.py:236
  384.3 2.5 add_convert_fusion
  (288 shorter events, 69.3 us)
Async XLA Ops:
  6.5 212.0 %all-gather.9.cloned.1.call-start = ((), (), s32[]{:S(2)}) async-start(), calls=%async_computation.2 | async-start | bytes 5242880 | tf_op jit(solution)/shard_map/all_gather | solution.py:220
  7.3 290.1 %all-gather.11.cloned.1.call-start = ((), (), s32[]{:S(2)}) async-start(), calls=%async_computation.3 | async-start | bytes 17842176 | tf_op jit(solution)/shard_map/all_gather | solution.py:19
  9.2 66.4 %copy-start = (bf16[1024,256]{1,0:T(8,128)(2,1)S(1)}, bf16[1024,256]{1,0:T(8,128)(2,1)}, u32[]{:S(2)}) copy-start(bf16[1024,256]{1,0:T(8,128)(2,1)} %param.16) | copy-start | bytes 1572868
  41.0 35.1 %copy-start.2 = (bf16[1024,256]{1,0:T(8,128)(2,1)S(1)}, bf16[1024,256]{1,0:T(8,128)(2,1)}, u32[]{:S(2)}) copy-start(bf16[1024,256]{1,0:T(8,128)(2,1)} %param.17) | copy-start | bytes 1572868
  43.7 34.0 %copy-start.6 = (f32[2,1024]{1,0:T(2,128)S(1)}, f32[2,1024]{1,0:T(2,128)}, u32[]{:S(2)}) copy-start(f32[2,1024]{1,0:T(2,128)} %param.19) | copy-start | bytes 24580
  43.7 34.0 %copy-start.8 = (u32[128]{0:T(128)S(1)}, u32[128]{0:T(128)}, u32[]{:S(2)}) copy-start(u32[128]{0:T(128)} %constant.134) | copy-start | bytes 1540
  72.4 0.8 copy-start.1
  76.1 24.0 %copy-start.3 = (f32[1,256,128]{2,1,0:T(8,128)S(1)}, f32[1,256,128]{2,1,0:T(8,128)}, u32[]{:S(2)}) copy-start(f32[1,256,128]{2,1,0:T(8,128)} %get-tuple-element.183) | copy-start | bytes 393220
  76.1 24.0 %copy-start.4 = (f32[1,256,128]{2,1,0:T(8,128)S(1)}, f32[1,256,128]{2,1,0:T(8,128)}, u32[]{:S(2)}) copy-start(f32[1,256,128]{2,1,0:T(8,128)} %get-tuple-element.184) | copy-start | bytes 393220
  76.1 24.0 %copy-start.5 = (f32[1,256,128]{2,1,0:T(8,128)S(1)}, f32[1,256,128]{2,1,0:T(8,128)}, u32[]{:S(2)}) copy-start(f32[1,256,128]{2,1,0:T(8,128)} %get-tuple-element.171) | copy-start | bytes 393220
  101.9 109.7 %copy-start.7 = (bf16[2048]{0:T(1024)(128)(2,1)S(1)}, bf16[2048]{0:T(1024)(128)(2,1)}, u32[]{:S(2)}) copy-start(bf16[2048]{0:T(1024)(128)(2,1)} %param.24) | copy-start | bytes 12292
  207.8 10.6 %all-to-all-start = ((bf16[4,256,256]{1,2,0:T(8,128)(2,1)}), bf16[4,256,256]{1,2,0:T(8,128)(2,1)S(1)}, u32[]{:S(2)}, u32[]{:S(2)}) async-start(bf16[4,256,256]{1,2,0:T(8,128)(2,1)} %bitcast.514), calls=%async_computation | async-start | bytes 1048576 | tf_op jit(solution)/shard_map/all_to_all | solution.py:217
  211.6 172.7 %reduce-scatter.2.cloned.1.call-start = ((), (), s32[]{:S(2)}) async-start(), calls=%async_computation.4 | async-start | bytes 5242880 | tf_op jit(solution)/shard_map/reduce_scatter | solution.py:236
  222.6 17.5 %collective-permute-start = (bf16[256,2048]{1,0:T(8,128)(2,1)S(1)}, bf16[256,2048]{1,0:T(8,128)(2,1)S(1)}, u32[]{:S(2)}, u32[]{:S(2)}) collective-permute-start(bf16[256,2048]{1,0:T(8,128)(2,1)S(1)} %multiply_convert_fusion.1), channel_id=1, source_target_pairs={{0,1},{1,2},{2,3},{3,0},{4,5},{5,6},{6,7},{7,4},{8,9},{9,10},{10,1... | collective-permute-start | bytes 3145736 | tf_op jit(solution)/shard_map/ppermute | solution.py:228
  240.1 21.7 %collective-permute-start.1 = (bf16[256,2048]{1,0:T(8,128)(2,1)S(1)}, bf16[256,2048]{1,0:T(8,128)(2,1)}, u32[]{:S(2)}, u32[]{:S(2)}) collective-permute-start(bf16[256,2048]{1,0:T(8,128)(2,1)S(1)} %collective-permute-done), channel_id=1, source_target_pairs={{0,1},{1,2},{2,3},{3,0},{4,5},{5,6},{6,7},{7,4},{8,9},{9,10},{10,1... | collective-permute-start | bytes 3145736 | tf_op jit(solution)/shard_map/ppermute | solution.py:228
  261.8 21.6 %collective-permute-start.2 = (bf16[256,2048]{1,0:T(8,128)(2,1)}, bf16[256,2048]{1,0:T(8,128)(2,1)}, u32[]{:S(2)}, u32[]{:S(2)}) collective-permute-start(bf16[256,2048]{1,0:T(8,128)(2,1)} %collective-permute-done.1), channel_id=1, source_target_pairs={{0,1},{1,2},{2,3},{3,0},{4,5},{5,6},{6,7},{7,4},{8,9},{9,10},{10,1... | collective-permute-start | bytes 3145736 | tf_op jit(solution)/shard_map/ppermute | solution.py:228
Sparse Core Ops, SparseCore 0:
  9.0 51.1 all-gather.8
  62.5 74.8 all-gather.10
  329.8 54.4 reduce-scatter.1
